TPU v7x, 32 devices: a whole 2x2x4 slice. The times are simulated.
32 devices in a mesh: sp: 8 (over z, core), tp: 4 (over y, x).
Axes of the slice: x: 2, y: 2, z: 4, core: 2. Of those that a mesh axis runs over, the one named last changes fastest.
Arguments:
- residual: bfloat16 [2048, 4096], P('sp', 'tp'), may hold values from -6 to 6
- pool_in: bfloat16 [2048, 2048], P('sp', 'tp'), may hold values from -6 to 6
- docs: int32 [2048], P('sp'), may hold values from 0 to 3, never falling along the last dimension, each value on 1 to 1024 neighbouring positions
- pool_weight: bfloat16 [16, 128, 128], P('tp'), may hold values from -0.5 to 0.5
- pool_gain: float32 [2048], P('tp'), may hold values from 0.1 to 1.9
- out_weight: bfloat16 [2048, 4096], P(None, 'tp'), may hold values from -0.125 to 0.125
- norm_gain: float32 [4096], replicated, may hold values from 0.1 to 1.9
- routes: int32 [2048, 2], P('sp'), may hold values from 0 to 7, all different within a row; in each aligned block of 256 rows (0 to 255, 256 to 511, ...) at most 96 rows name the same one
- route_weights: float32 [2048, 2], P('sp'), may hold values from 0.25 to 1
- w_gate: bfloat16 [8, 4096, 2048], P('sp', None, 'tp'), may hold values from -0.09375 to 0.09375
- w_up: bfloat16 [8, 4096, 2048], P('sp', None, 'tp'), may hold values from -0.09375 to 0.09375
- w_down: bfloat16 [8, 2048, 4096], P('sp', None, 'tp'), may hold values from -0.125 to 0.125
Outputs:
- layer_out: bfloat16 [2048, 4096], P('sp', 'tp')
Inputs may be any that keep to these rules, and one draw needn't show every extreme that they name: `docs`: document numbers never fall along the sequence; each document has at most 1024 positions. `routes`: each token names 2 different experts; among the tokens of one index of sp (aligned blocks of 256 rows) no expert is named more than 96 times, a bound that some block reaches.
All inputs are finite; a program needn't handle non-finite values.
Results may differ from a plain program's by a relative error of at most 0.012.
Values may be sent and summed in bfloat16 or wider, within the bound.
A program may use at most 64 MiB of HBM per device.

v0:
```python
import jax
import jax.numpy as jnp
from jax import lax
from jax.sharding import PartitionSpec as P

GD = 128
TOPK = 2
EXP_DEV = 1


EPS = 1e-06


def shifted_2(shard, axis, by):
    size = lax.axis_size(axis)
    pairs = [(i, i + by) for i in range(size) if 0 <= i + by < size]
    return lax.ppermute(shard, axis, pairs)


def shards(
    residual,
    pool_in,
    docs,
    pool_weight,
    pool_gain,
    out_weight,
    norm_gain,
    routes,
    route_weights,
    w_gate,
    w_up,
    w_down,
):
    length = pool_in.shape[0]
    width_loc = pool_in.shape[1]
    sp_index = lax.axis_index("sp")
    tp_index = lax.axis_index("tp")
    n_sp = lax.axis_size("sp")
    n_tp = lax.axis_size("tp")
    reach = 15
    prev_rows, prev_docs = shifted_2(
        (pool_in[length - reach :], docs[length - reach :].astype(jnp.bfloat16)), "sp", 1
    )
    extended = jnp.concatenate([prev_rows, pool_in], axis=0).astype(jnp.float32)
    ext_docs = jnp.concatenate([prev_docs.astype(jnp.float32), docs.astype(jnp.float32)])
    own_docs = docs.astype(jnp.float32)
    places = sp_index * length + jnp.arange(length)
    groups_loc = width_loc // GD
    group_of = tp_index * groups_loc + jnp.arange(width_loc) // GD
    span = 2 ** (1 + group_of % 4)
    totals = jnp.zeros((length, width_loc), jnp.float32)
    counts = jnp.zeros((length, width_loc), jnp.float32)
    for offset in range(16):
        shifted = extended[reach - offset : reach - offset + length]
        prior = ext_docs[reach - offset : reach - offset + length]
        same = ((places >= offset) & (prior == own_docs)).astype(jnp.float32)[:, None]
        weight = same * (offset < span).astype(jnp.float32)[None, :]
        totals = totals + weight * shifted
        counts = counts + weight
    diff = (totals / counts - extended[reach:]).astype(jnp.bfloat16)
    mixed = jnp.einsum(
        "tgc,gcd->tgd",
        diff.reshape(length, groups_loc, GD),
        pool_weight,
        preferred_element_type=jnp.float32,
    )
    pooled = (mixed.reshape(length, width_loc) * pool_gain).astype(jnp.bfloat16)
    block = out_weight
    proj = jnp.dot(
        lax.all_gather(pooled, "tp", axis=1, tiled=True), block, preferred_element_type=jnp.float32
    )
    updated = (residual.astype(jnp.float32) + proj).astype(jnp.bfloat16)
    upf = updated.astype(jnp.float32)
    cols = residual.shape[1]
    model_width = cols * n_tp
    experts = n_sp * EXP_DEV
    slots_cap = length * TOPK * 3 // (2 * experts)
    ids = routes.reshape(-1)
    onehot = (ids[:, None] == jnp.arange(experts)[None, :]).astype(jnp.int32)
    rank = jnp.sum(onehot * (jnp.cumsum(onehot, axis=0) - 1), axis=1)
    slot = ids * slots_cap + rank
    source = jnp.arange(length * TOPK) // TOPK
    squares = lax.psum(jnp.sum(upf * upf, axis=1), "tp")
    gain_cols = lax.dynamic_slice_in_dim(norm_gain, tp_index * cols, cols, 0)
    normed = (upf * lax.rsqrt(squares / model_width + EPS)[:, None] * gain_cols).astype(
        jnp.bfloat16
    )
    send = jnp.zeros((experts * slots_cap, cols), jnp.bfloat16).at[slot].set(normed[source])
    arrived = lax.all_to_all(
        send.reshape(experts, slots_cap, cols), "sp", split_axis=0, concat_axis=0, tiled=True
    )
    part_rows = arrived.reshape(-1, cols)
    piece = lax.all_gather(part_rows, "tp", axis=1, tiled=True)
    gate_block = w_gate[0]
    up_block = w_up[0]
    gate = jnp.dot(piece, gate_block, preferred_element_type=jnp.float32)
    up = jnp.dot(piece, up_block, preferred_element_type=jnp.float32)
    act = (jax.nn.silu(gate) * up).astype(jnp.bfloat16)
    block = w_down[0]
    produced = jnp.dot(
        lax.all_gather(act, "tp", axis=1, tiled=True), block, preferred_element_type=jnp.float32
    ).astype(jnp.bfloat16)
    returned = lax.all_to_all(
        produced.reshape(n_sp, slots_cap, cols), "sp", split_axis=0, concat_axis=0, tiled=True
    )
    picked = returned.reshape(-1, cols)[slot].reshape(length, TOPK, cols)
    combined = upf + jnp.sum(route_weights[:, :, None] * picked.astype(jnp.float32), axis=1)
    return combined.astype(jnp.bfloat16)


def solution(mesh):
    placed = (
        P("sp", "tp"),
        P("sp", "tp"),
        P("sp"),
        P("tp", None, None),
        P("tp"),
        P(None, "tp"),
        P(),
        P("sp", None),
        P("sp", None),
        P("sp", None, "tp"),
        P("sp", None, "tp"),
        P("sp", None, "tp"),
    )
    return jax.shard_map(
        shards, mesh=mesh, in_specs=placed, out_specs=P("sp", "tp"), check_vma=False
    )
```

profile of v0, /device:TPU:0, one launch (start us, length us, event | category | flops | bytes accessed | tf_op | source)
XLA Modules:
  0.0 298.0 jit_solution(6181939409803868553)
XLA Ops:
  6.5 0.8 fusion.51
  7.3 0.1 slice.109
  7.4 2.4 collective-permute-start.1
  9.8 0.7 slice.107
  10.5 4.6 %collective-permute-start = (bf16[15,512]{1,0:T(8,128)(2,1)S(1)}, bf16[15,512]{1,0:T(8,128)(2,1)S(1)}, u32[]{:S(2)}, u32[]{:S(2)}) collective-permute-start(bf16[15,512]{1,0:T(8,128)(2,1)S(1)} %slice.107), channel_id=1, source_target_pairs={{0,4},{4,8},{8,12},{12,16},{16,20},{20,24},{24,28},{1,5},{5,9},{9,... | collective-permute-start | bytes 46088 | tf_op jit(solution)/shard_map/ppermute | solution.py:17
  15.3 0.1 pad_maximum_fusion
  15.4 0.8 and_convert_fusion.14
  16.2 1.0 maximum_convert_fusion
  17.2 0.0 copy-start.4
  17.2 0.0 copy-start.3
  17.2 0.0 copy-start.8
  17.2 2.2 fusion.38
  19.5 0.8 fusion.36
  20.3 0.0 all-gather.4.cloned.1.call-update
  20.3 0.0 all-gather.6.cloned.1.call-start
  20.4 0.1 copy.20
  20.5 0.1 eq.95
  20.7 0.1 eq.91
  20.8 1.1 reduce-window.6
  22.0 0.2 slice_reduce_fusion
  22.3 0.1 copy.19
  22.4 0.1 mul.619
  22.6 0.1 fusion.42
  22.7 0.0 dynamic-slice-start
  22.7 26.0 %all-gather.4.cloned.1.call-done = bf16[256,2048]{0,1:T(8,128)(2,1)} async-done(((bf16[256,512]{0,1:T(8,128)(2,1)}), bf16[256,2048]{0,1:T(8,128)(2,1)}) %all-gather.4.cloned.1.call-update) | async-done | bytes 1048592 | tf_op jit(solution)/shard_map/all_gather | solution.py:70
  48.7 3.9 %fusion.12 = (f32[256]{0:T(256)S(1)}, bf16[256,1024]{1,0:T(8,128)(2,1)S(1)}) fusion(bf16[256,2048]{0,1:T(8,128)(2,1)} %all-gather.4.cloned.1.call-done, bf16[2048,1024]{1,0:T(8,128)(2,1)} %param.17, bf16[256,1024]{1,0:T(8,128)(2,1)S(1)} %copy-done.8), kind=kOutput, calls=%fused_computation.17 | convolution fusion | flops 1075314432 | bytes 6292480 | tf_op jit(solution)/shard_map/dot_general | solution.py:69
  52.5 0.0 copy-start.1
  52.6 8.9 %psum.7 = f32[256]{0:T(256)S(1)} all-reduce(f32[256]{0:T(256)S(1)} %get-tuple-element.23), channel_id=1, replica_groups=mesh['sp'=8,'tp'=4] {'tp'}, use_global_device_ids=true, to_apply=%region_4.5 | all-reduce | flops 256 | bytes 2048 | tf_op jit(solution)/shard_map/psum | solution.py:83
  61.5 0.2 fusion.14
  61.7 6.6 %scatter_custom_fusion = bf16[768,1024]{1,0:T(8,128)(2,1)S(1)} fusion(s32[512]{0:T(512)S(1)} %bitcast.48, bf16[256,1024]{1,0:T(8,128)(2,1)S(1)} %fusion.14, s32[1024]{0:T(1024)S(1)} %pad_clamp_fusion.1, bf16[]{:T(256)} %constant.159.clone.1), kind=kCustom, calls=%fused_computation.21 | custom fusion | bytes 1572866 | tf_op jit(solution)/shard_map/scatter | solution.py:88
  68.3 42.3 %all_to_all.10 = bf16[8,96,1024]{2,1,0:T(8,128)(2,1)} all-to-all(bf16[8,96,1024]{2,1,0:T(8,128)(2,1)S(1)} %bitcast.47), channel_id=1, replica_groups=mesh['sp'=8,'tp'=4] {'sp'}, dimensions={0} | all-to-all | bytes 3145728 | tf_op jit(solution)/shard_map/all_to_all | solution.py:89
  110.7 0.0 all-gather.6.cloned.1.call-update
  110.7 0.2 all-gather.8.cloned.1.call-start
  110.9 67.9 %all-gather.6.cloned.1.call-done = bf16[768,4096]{1,0:T(8,128)(2,1)} async-done(((bf16[768,1024]{1,0:T(8,128)(2,1)}), bf16[768,4096]{1,0:T(8,128)(2,1)}) %all-gather.6.cloned.1.call-update) | async-done | bytes 6291472 | tf_op jit(solution)/shard_map/all_gather | solution.py:93
  178.8 6.9 %fusion.4 = f32[768,512]{1,0:T(8,128)S(1)} fusion(bf16[768,4096]{1,0:T(8,128)(2,1)} %all-gather.6.cloned.1.call-done, bf16[1,4096,512]{2,1,0:T(8,128)(2,1)} %param.21), kind=kOutput, calls=%fused_computation.7 | convolution fusion | flops 3221225472 | bytes 12058624 | tf_op jit(solution)/shard_map/dot_general | solution.py:96
  185.7 0.1 copy-done.7
  185.8 4.5 %multiply_convert_fusion = bf16[768,512]{1,0:T(8,128)(2,1)} fusion(f32[768,512]{1,0:T(8,128)S(1)} %fusion.4, bf16[768,4096]{1,0:T(8,128)(2,1)S(1)} %copy-done.6, bf16[1,4096,512]{2,1,0:T(8,128)(2,1)S(1)} %copy-done.7), kind=kOutput, calls=%fused_computation.11 | convolution fusion | flops 3223584768 | bytes 12845056 | tf_op jit(solution)/shard_map/dot_general | solution.py:97
  190.3 0.0 all-gather.8.cloned.1.call-update
  190.3 43.9 %all-gather.8.cloned.1.call-done = bf16[768,2048]{1,0:T(8,128)(2,1)} async-done(((bf16[768,512]{1,0:T(8,128)(2,1)}), bf16[768,2048]{1,0:T(8,128)(2,1)}) %all-gather.8.cloned.1.call-update) | async-done | bytes 3145744 | tf_op jit(solution)/shard_map/all_gather | solution.py:101
  234.2 7.7 %fusion.6 = bf16[768,1024]{1,0:T(8,128)(2,1)} fusion(bf16[768,2048]{1,0:T(8,128)(2,1)} %all-gather.8.cloned.1.call-done, bf16[1,2048,1024]{2,1,0:T(8,128)(2,1)} %param.23), kind=kOutput, calls=%fused_computation.10 | convolution fusion | flops 3222011904 | bytes 8912896 | tf_op jit(solution)/shard_map/dot_general | solution.py:100
  241.9 4.7 %all-to-all-start.1 = ((bf16[8,96,1024]{2,1,0:T(8,128)(2,1)}), bf16[8,96,1024]{2,1,0:T(8,128)(2,1)S(1)}, u32[]{:S(2)}, u32[]{:S(2)}) async-start(bf16[8,96,1024]{2,1,0:T(8,128)(2,1)} %bitcast.12), calls=%async_computation.1 | async-start | bytes 3145728 | tf_op jit(solution)/shard_map/all_to_all | solution.py:103
  246.6 0.1 copy.18
  246.8 37.6 %all-to-all-done.1 = bf16[8,96,1024]{2,1,0:T(8,128)(2,1)S(1)} async-done(((bf16[8,96,1024]{2,1,0:T(8,128)(2,1)}), bf16[8,96,1024]{2,1,0:T(8,128)(2,1)S(1)}, u32[]{:S(2)}, u32[]{:S(2)}) %all-to-all-start.1) | async-done | bytes 1572896 | tf_op jit(solution)/shard_map/all_to_all | solution.py:103
  284.4 2.0 gather_fusion
  286.5 1.3 reshape.255
  287.9 0.0 copy-start.2
  287.9 2.6 multiply_reduce_fusion
  290.5 0.9 fusion.15
  (34 shorter events, 0.3 us)
Async XLA Ops:
  6.5 10.7 %copy-start = (bf16[4,128,128]{2,1,0:T(8,128)(2,1)S(1)}, bf16[4,128,128]{2,1,0:T(8,128)(2,1)}, u32[]{:S(2)}) copy-start(bf16[4,128,128]{2,1,0:T(8,128)(2,1)} %param.15) | copy-start | bytes 393220
  6.5 42.1 %all-gather.4.cloned.1.call-start = ((), (), s32[]{:S(2)}) async-start(), calls=%async_computation.2 | async-start | bytes 1310720 | tf_op jit(solution)/shard_map/all_gather | solution.py:70
  7.4 7.9 %collective-permute-start.1 = (bf16[15]{0:T(256)(128)(2,1)S(1)}, bf16[15]{0:T(256)(128)(2,1)S(1)}, u32[]{:S(2)}, u32[]{:S(2)}) collective-permute-start(bf16[15]{0:T(256)(128)(2,1)S(1)} %slice.109), channel_id=1, source_target_pairs={{0,4},{4,8},{8,12},{12,16},{16,20},{20,24},{24,28},{1,5},{5,9},{9,... | collective-permute-start | bytes 98 | tf_op jit(solution)/shard_map/ppermute | solution.py:17
  10.5 5.7 %collective-permute-start = (bf16[15,512]{1,0:T(8,128)(2,1)S(1)}, bf16[15,512]{1,0:T(8,128)(2,1)S(1)}, u32[]{:S(2)}, u32[]{:S(2)}) collective-permute-start(bf16[15,512]{1,0:T(8,128)(2,1)S(1)} %slice.107), channel_id=1, source_target_pairs={{0,4},{4,8},{8,12},{12,16},{16,20},{20,24},{24,28},{1,5},{5,9},{9,... | collective-permute-start | bytes 46088 | tf_op jit(solution)/shard_map/ppermute | solution.py:17
  17.2 2.3 copy-start.4
  17.2 3.2 %copy-start.3 = (s32[256,2]{0,1:T(2,128)S(1)}, s32[256,2]{0,1:T(2,128)}, u32[]{:S(2)}) copy-start(s32[256,2]{0,1:T(2,128)} %param.19) | copy-start | bytes 6148
  17.2 31.4 %copy-start.8 = (bf16[256,1024]{1,0:T(8,128)(2,1)S(1)}, bf16[256,1024]{1,0:T(8,128)(2,1)}, u32[]{:S(2)}) copy-start(bf16[256,1024]{1,0:T(8,128)(2,1)} %param.12) | copy-start | bytes 1572868
  20.3 158.5 %all-gather.6.cloned.1.call-start = ((), (), s32[]{:S(2)}) async-start(), calls=%async_computation.3 | async-start | bytes 7864320 | tf_op jit(solution)/shard_map/all_gather | solution.py:93
  22.7 38.8 %dynamic-slice-start = ((f32[4096]{0:T(1024)}, s32[]{:T(128)}), f32[1024]{0:T(1024)S(1)}, s32[]{:S(2)}) async-start(f32[4096]{0:T(1024)} %param.18, s32[]{:T(128)} %select_n.469), calls=%async_computation.5 | async-start | bytes 8704 | tf_op jit(solution)/shard_map/dynamic_slice | solution.py:84
  52.5 9.2 %copy-start.1 = (bf16[256,1024]{1,0:T(8,128)(2,1)}, bf16[256,1024]{1,0:T(8,128)(2,1)S(1)}, u32[]{:S(2)}) copy-start(bf16[256,1024]{1,0:T(8,128)(2,1)S(1)} %get-tuple-element.24) | copy-start | bytes 1572868
  110.7 123.5 %all-gather.8.cloned.1.call-start = ((), (), s32[]{:S(2)}) async-start(), calls=%async_computation.4 | async-start | bytes 3932160 | tf_op jit(solution)/shard_map/all_gather | solution.py:101
  178.8 6.9 %copy-start.6 = (bf16[768,4096]{1,0:T(8,128)(2,1)S(1)}, bf16[768,4096]{1,0:T(8,128)(2,1)}, u32[]{:S(2)}) copy-start(bf16[768,4096]{1,0:T(8,128)(2,1)} %all-gather.6.cloned.1.call-done) | copy-start | bytes 18874372
  178.8 7.0 %copy-start.7 = (bf16[1,4096,512]{2,1,0:T(8,128)(2,1)S(1)}, bf16[1,4096,512]{2,1,0:T(8,128)(2,1)}, u32[]{:S(2)}) copy-start(bf16[1,4096,512]{2,1,0:T(8,128)(2,1)} %param.22) | copy-start | bytes 12582916
  241.9 4.7 %copy-start.5 = (f32[256,2]{0,1:T(2,128)S(1)}, f32[256,2]{0,1:T(2,128)}, u32[]{:S(2)}) copy-start(f32[256,2]{0,1:T(2,128)} %param.20) | copy-start | bytes 6148
  241.9 42.5 %all-to-all-start.1 = ((bf16[8,96,1024]{2,1,0:T(8,128)(2,1)}), bf16[8,96,1024]{2,1,0:T(8,128)(2,1)S(1)}, u32[]{:S(2)}, u32[]{:S(2)}) async-start(bf16[8,96,1024]{2,1,0:T(8,128)(2,1)} %bitcast.12), calls=%async_computation.1 | async-start | bytes 3145728 | tf_op jit(solution)/shard_map/all_to_all | solution.py:103
  287.9 2.7 copy-start.2
Sparse Core Ops, SparseCore 0:
  20.5 28.1 all-gather.3
  110.8 67.9 all-gather.5
  190.4 43.7 all-gather.7
where the time goes:
time: 298 us
  waiting for transfers between devices  175 us (59%)
  blocking collectives  51.2 us (17%)
  matrix products  25.1 us (8%)
  between operations  13.4 us (4%)
  local copies, waits for them, and re-layouts  12.1 us (4%)
  starting transfers between devices  12 us (4%)
  other arithmetic  8.74 us (3%)
    all_gather x1, waiting for transfers between devices, shards(): piece = lax.all_gather(part_rows, 'tp', axis=1, tiled=True)  67.9 us
    all_gather x1, waiting for transfers between devices, shards(): lax.all_gather(act, 'tp', axis=1, tiled=True)  43.9 us
    all_to_all x1, blocking collectives, shards(): lax.all_to_all(send.reshape(experts, slots_cap, cols), 'sp', split_axis=0...  42.3 us
    all_to_all x1, waiting for transfers between devices, shards(): lax.all_to_all(produced.reshape(n_sp, slots_cap, cols), 'sp', split_axis=...  37.6 us
    all_gather x1, waiting for transfers between devices, shards(): lax.all_gather(pooled, 'tp', axis=1, tiled=True)  26 us
    psum x1, blocking collectives, shards(): squares = lax.psum(jnp.sum(upf * upf, axis=1), 'tp')  8.94 us
    dot_general x1, matrix products, shards(): jnp.dot(lax.all_gather(act, 'tp', axis=1, tiled=True), block, preferred_e...  7.7 us
    ppermute x2, starting transfers between devices, shifted_2(): return lax.ppermute(shard, axis, pairs)  6.96 us
  transfers between devices with their start and end apart: 6, of which 4 were waited for; matrix products, arithmetic and copies ran while one was open for 1% of the time, Pallas kernels for 0%

commit v1 on v0

v1 whole, which is shorter than its diff:
```python
import functools

import jax
import jax.numpy as jnp
from jax import lax
from jax.experimental import pallas as pl
from jax.experimental.pallas import tpu as pltpu
from jax.sharding import PartitionSpec as P

GD = 128
TOPK = 2
EXP_DEV = 1


EPS = 1e-06


def shifted_2(shard, axis, by):
    size = lax.axis_size(axis)
    pairs = [(i, i + by) for i in range(size) if 0 <= i + by < size]
    return lax.ppermute(shard, axis, pairs)


MESH = pl.DeviceIdType.MESH
CORES = 2


def remote(src, dst, send_sem, recv_sem, device):
    return pltpu.make_async_remote_copy(
        src_ref=src,
        dst_ref=dst,
        send_sem=send_sem,
        recv_sem=recv_sem,
        device_id=device,
        device_id_type=MESH,
    )


def greet(devices):
    barrier = pltpu.get_barrier_semaphore()
    for device in devices:
        pl.semaphore_signal(barrier, inc=1, device_id=device, device_id_type=MESH)
    pl.semaphore_wait(barrier, len(devices))


def project_kernel(
    n_tp,
    pooled,
    residual,
    gain,
    weight_hbm,
    updated,
    normed,
    gathered,
    weight,
    mine,
    sums,
    weight_sem,
    send_sem,
    recv_sem,
    sums_send,
    sums_recv,
):
    sp, tp = lax.axis_index("sp"), lax.axis_index("tp")
    width = pooled.shape[1]
    cols = residual.shape[1]
    load = pltpu.make_async_copy(weight_hbm, weight, weight_sem)
    load.start()
    peers = [lax.rem(tp + j, n_tp) for j in range(1, n_tp)]
    greet([(sp, peer) for peer in peers])
    sends = []
    for j, peer in enumerate(peers):
        sends.append(
            remote(pooled, gathered.at[tp], send_sem.at[j], recv_sem.at[tp], (sp, peer))
        )
        sends[-1].start()
    load.wait()

    def part(block, owner):
        rows = weight[pl.ds(pl.multiple_of(owner * width, width), width), :]
        return jnp.dot(block, rows, preferred_element_type=jnp.float32)

    total = part(pooled[...], tp)
    for j in range(1, n_tp):
        owner = lax.rem(tp + n_tp - j, n_tp)
        remote(
            pooled, gathered.at[owner], send_sem.at[0], recv_sem.at[owner], (sp, owner)
        ).wait_recv()
        total = total + part(gathered[owner], owner)
    new = (residual[...].astype(jnp.float32) + total).astype(jnp.bfloat16)
    updated[...] = new
    upf = new.astype(jnp.float32)
    squares = jnp.sum(upf * upf, axis=1, keepdims=True)
    own = jnp.broadcast_to(squares, (squares.shape[0], 128)).T[0:8]
    mine[...] = own
    small = []
    for j, peer in enumerate(peers):
        small.append(
            remote(mine, sums.at[tp], sums_send.at[j], sums_recv.at[tp], (sp, peer))
        )
        small[-1].start()
    for j in range(1, n_tp):
        owner = lax.rem(tp + n_tp - j, n_tp)
        remote(
            mine, sums.at[owner], sums_send.at[0], sums_recv.at[owner], (sp, owner)
        ).wait_recv()
        own = own + sums[owner]
    scale = lax.rsqrt(own / (cols * n_tp) + EPS)
    column = jnp.broadcast_to(scale[0:1], (128, scale.shape[1])).T[:, 0:1]
    normed[...] = (upf * column * gain[...]).astype(jnp.bfloat16)
    for copy in sends + small:
        copy.wait_send()


def experts_kernel(
    n_sp,
    n_tp,
    send,
    gate_hbm,
    up_hbm,
    down_hbm,
    out,
    rows,
    act,
    prod,
    w_gate,
    w_up,
    w_down,
    load_sem,
    d_send,
    d_recv,
    f_send,
    f_recv,
    a_send,
    a_recv,
    r_send,
    r_recv,
):
    sp, tp = lax.axis_index("sp"), lax.axis_index("tp")
    chips = n_sp // CORES
    my_chip, my_core = sp // CORES, sp % CORES
    cap, cols = send.shape[2], send.shape[3]
    hidden = act.shape[4]
    relay = n_tp == 4
    flat = CORES * cap

    loads = [
        pltpu.make_async_copy(gate_hbm, w_gate, load_sem.at[0]),
        pltpu.make_async_copy(up_hbm, w_up, load_sem.at[1]),
        pltpu.make_async_copy(down_hbm, w_down, load_sem.at[2]),
    ]
    for copy in loads:
        copy.start()
    greet(
        [(lax.rem(sp + j, n_sp), tp) for j in range(1, n_sp)]
        + [(sp, lax.rem(tp + j, n_tp)) for j in range(1, n_tp)]
    )

    def turn(k):
        odd = k % 2
        return (odd * ((k + 1) // 2) + (1 - odd) * (chips - k // 2)) % chips

    def dispatch(chip, core):
        return remote(
            send.at[chip, core],
            rows.at[my_chip, tp, my_core],
            d_send.at[chip * CORES + core],
            d_recv.at[sp],
            (chip * CORES + core, tp),
        )

    own = pltpu.make_async_copy(
        send.at[my_chip, my_core], rows.at[my_chip, tp, my_core], d_recv.at[sp]
    )
    own.start()
    dispatch(my_chip, 1 - my_core).start()

    @pl.loop(1, chips)
    def _(k):
        chip = (my_chip + turn(k)) % chips
        for core in range(CORES):
            dispatch(chip, core).start()

    def spread(buf, chip, ssem, rsem):
        if relay:
            near = (2 * (tp // 2) + 1 - tp % 2, (tp + 2) % 4)
        else:
            near = [(tp + j) % n_tp for j in range(1, n_tp)]
        return [
            remote(buf.at[chip, tp], buf.at[chip, tp], ssem.at[chip, j], rsem.at[chip, tp], (sp, peer))
            for j, peer in enumerate(near)
        ]

    across = 2 * (tp // 2) + 1 - tp % 2
    along = (tp + 2) % 4

    def relays(buf, chip, ssem, rsem):
        return [
            remote(
                buf.at[chip, across, 0],
                buf.at[chip, across, 0],
                ssem.at[chip, 2],
                rsem.at[chip, n_tp],
                (sp, along),
            ),
            remote(
                buf.at[chip, along, 1],
                buf.at[chip, along, 1],
                ssem.at[chip, 3],
                rsem.at[chip, n_tp + 1],
                (sp, across),
            ),
        ]

    def arrive(buf, chip, peer, ssem, rsem):
        remote(
            buf.at[chip, peer], buf.at[chip, peer], ssem.at[chip, 0], rsem.at[chip, peer], (sp, peer)
        ).wait_recv()

    def pass_on(buf, chip, ssem, rsem):
        if relay:
            first, second = relays(buf, chip, ssem, rsem)
            arrive(buf, chip, across, ssem, rsem)
            first.start()
            arrive(buf, chip, along, ssem, rsem)
            second.start()

    def complete(buf, chip, ssem, rsem):
        if relay:
            far = 3 - tp
            for half, peer in ((0, along), (1, across)):
                remote(
                    buf.at[chip, far, half],
                    buf.at[chip, far, half],
                    ssem.at[chip, 0],
                    rsem.at[chip, n_tp + half],
                    (sp, peer),
                ).wait_recv()
        else:
            for j in range(1, n_tp):
                arrive(buf, chip, (tp + j) % n_tp, ssem, rsem)

    def source(k):
        return (my_chip + chips - turn(k)) % chips

    def give_back(chip, core):
        return remote(
            prod.at[chip, core],
            out.at[my_chip, my_core],
            r_send.at[chip * CORES + core],
            r_recv.at[sp],
            (chip * CORES + core, tp),
        )

    tile = min(hidden, 256)
    wide = min(cols, 256)

    @pl.loop(0, chips + 4)
    def _(i):
        @pl.when(i < chips)
        def _():
            chip = source(i)
            for core in range(CORES):
                remote(
                    send.at[chip, core],
                    rows.at[chip, tp, core],
                    d_send.at[0],
                    d_recv.at[chip * CORES + core],
                    (sp, tp),
                ).wait_recv()
            for copy in spread(rows, chip, f_send, f_recv):
                copy.start()

        @pl.when((i >= 1) & (i < chips + 1))
        def _():
            pass_on(rows, source(i - 1), f_send, f_recv)

        @pl.when(i == 2)
        def _():
            for copy in loads:
                copy.wait()

        @pl.when((i >= 2) & (i < chips + 2))
        def _():
            chip = source(i - 2)
            complete(rows, chip, f_send, f_recv)

            @pl.loop(0, hidden // tile)
            def _(n):
                at = pl.ds(pl.multiple_of(n * tile, tile), tile)
                gate = jnp.zeros((flat, tile), jnp.float32)
                up = jnp.zeros((flat, tile), jnp.float32)
                for t in range(n_tp):
                    block = rows[chip, t].reshape(flat, cols)
                    deep = pl.ds(t * cols, cols)
                    gate += jnp.dot(block, w_gate[deep, at], preferred_element_type=jnp.float32)
                    up += jnp.dot(block, w_up[deep, at], preferred_element_type=jnp.float32)
                value = (jax.nn.silu(gate) * up).astype(jnp.bfloat16)
                act[chip, tp, :, :, at] = value.reshape(CORES, cap, tile)

            for copy in spread(act, chip, a_send, a_recv):
                copy.start()

        @pl.when((i >= 3) & (i < chips + 3))
        def _():
            pass_on(act, source(i - 3), a_send, a_recv)

        @pl.when(i >= 4)
        def _():
            chip = source(i - 4)
            complete(act, chip, a_send, a_recv)

            @pl.loop(0, cols // wide)
            def _(n):
                at = pl.ds(pl.multiple_of(n * wide, wide), wide)
                total = jnp.zeros((flat, wide), jnp.float32)
                for t in range(n_tp):
                    block = act[chip, t].reshape(flat, hidden)
                    total += jnp.dot(
                        block, w_down[pl.ds(t * hidden, hidden), at], preferred_element_type=jnp.float32
                    )
                prod[chip, :, :, at] = total.astype(jnp.bfloat16).reshape(CORES, cap, wide)

            @pl.when(i == 4)
            def _():
                pltpu.make_async_copy(
                    prod.at[my_chip, my_core], out.at[my_chip, my_core], r_recv.at[sp]
                ).start()
                give_back(my_chip, 1 - my_core).start()

            @pl.when(i > 4)
            def _():
                for core in range(CORES):
                    give_back(chip, core).start()

    dispatch(my_chip, 1 - my_core).wait_send()
    give_back(my_chip, 1 - my_core).wait_send()

    @pl.loop(1, chips)
    def _(k):
        chip = (my_chip + turn(k)) % chips
        for core in range(CORES):
            dispatch(chip, core).wait_send()
            give_back(chip, core).wait_send()

    @pl.loop(0, chips)
    def _(chip):
        for buf, ssem, rsem in ((rows, f_send, f_recv), (act, a_send, a_recv)):
            for copy in spread(buf, chip, ssem, rsem):
                copy.wait_send()
            if relay:
                for copy in relays(buf, chip, ssem, rsem):
                    copy.wait_send()
        for core in range(CORES):
            remote(
                prod.at[chip, core],
                out.at[chip, core],
                r_send.at[0],
                r_recv.at[chip * CORES + core],
                (sp, tp),
            ).wait_recv()


VMEM_LIMIT = 60 * 1024 * 1024


def project(pooled, residual, gain, weight):
    n_tp = lax.axis_size("tp")
    length, cols = residual.shape
    dma = pltpu.SemaphoreType.DMA
    vmem = pl.BlockSpec(memory_space=pltpu.VMEM)
    return pl.pallas_call(
        functools.partial(project_kernel, n_tp),
        out_shape=[jax.ShapeDtypeStruct((length, cols), jnp.bfloat16)] * 2,
        in_specs=[vmem, vmem, vmem, pl.BlockSpec(memory_space=pl.ANY)],
        out_specs=[vmem, vmem],
        scratch_shapes=[
            pltpu.VMEM((n_tp, *pooled.shape), jnp.bfloat16),
            pltpu.VMEM(weight.shape, jnp.bfloat16),
            pltpu.VMEM((8, length), jnp.float32),
            pltpu.VMEM((n_tp, 8, length), jnp.float32),
            dma,
            dma((n_tp,)),
            dma((n_tp,)),
            dma((n_tp,)),
            dma((n_tp,)),
        ],
        compiler_params=pltpu.CompilerParams(
            collective_id=0, has_side_effects=True, vmem_limit_bytes=VMEM_LIMIT
        ),
    )(pooled, residual, gain, weight)


def run_experts(send, w_gate, w_up, w_down):
    n_sp, n_tp = lax.axis_size("sp"), lax.axis_size("tp")
    chips, _, cap, cols = send.shape
    hidden = w_gate.shape[1]
    dma = pltpu.SemaphoreType.DMA
    vmem = pl.BlockSpec(memory_space=pltpu.VMEM)
    hbm = pl.BlockSpec(memory_space=pl.ANY)
    return pl.pallas_call(
        functools.partial(experts_kernel, n_sp, n_tp),
        out_shape=jax.ShapeDtypeStruct(send.shape, jnp.bfloat16),
        in_specs=[vmem, hbm, hbm, hbm],
        out_specs=vmem,
        scratch_shapes=[
            pltpu.VMEM((chips, n_tp, CORES, cap, cols), jnp.bfloat16),
            pltpu.VMEM((chips, n_tp, CORES, cap, hidden), jnp.bfloat16),
            pltpu.VMEM(send.shape, jnp.bfloat16),
            pltpu.VMEM(w_gate.shape, jnp.bfloat16),
            pltpu.VMEM(w_up.shape, jnp.bfloat16),
            pltpu.VMEM(w_down.shape, jnp.bfloat16),
            dma((3,)),
            dma((n_sp,)),
            dma((n_sp,)),
            dma((chips, n_tp)),
            dma((chips, n_tp + 2)),
            dma((chips, n_tp)),
            dma((chips, n_tp + 2)),
            dma((n_sp,)),
            dma((n_sp,)),
        ],
        compiler_params=pltpu.CompilerParams(
            collective_id=1, has_side_effects=True, vmem_limit_bytes=VMEM_LIMIT
        ),
    )(send, w_gate, w_up, w_down)


def shards(
    residual,
    pool_in,
    docs,
    pool_weight,
    pool_gain,
    out_weight,
    norm_gain,
    routes,
    route_weights,
    w_gate,
    w_up,
    w_down,
):
    length = pool_in.shape[0]
    width_loc = pool_in.shape[1]
    sp_index = lax.axis_index("sp")
    tp_index = lax.axis_index("tp")
    n_sp = lax.axis_size("sp")
    n_tp = lax.axis_size("tp")
    reach = 15
    prev_rows, prev_docs = shifted_2(
        (pool_in[length - reach :], docs[length - reach :].astype(jnp.bfloat16)), "sp", 1
    )
    extended = jnp.concatenate([prev_rows, pool_in], axis=0).astype(jnp.float32)
    ext_docs = jnp.concatenate([prev_docs.astype(jnp.float32), docs.astype(jnp.float32)])
    own_docs = docs.astype(jnp.float32)
    places = sp_index * length + jnp.arange(length)
    groups_loc = width_loc // GD
    group_of = tp_index * groups_loc + jnp.arange(width_loc) // GD
    span = 2 ** (1 + group_of % 4)
    totals = jnp.zeros((length, width_loc), jnp.float32)
    counts = jnp.zeros((length, width_loc), jnp.float32)
    for offset in range(16):
        shifted = extended[reach - offset : reach - offset + length]
        prior = ext_docs[reach - offset : reach - offset + length]
        same = ((places >= offset) & (prior == own_docs)).astype(jnp.float32)[:, None]
        weight = same * (offset < span).astype(jnp.float32)[None, :]
        totals = totals + weight * shifted
        counts = counts + weight
    diff = (totals / counts - extended[reach:]).astype(jnp.bfloat16)
    mixed = jnp.einsum(
        "tgc,gcd->tgd",
        diff.reshape(length, groups_loc, GD),
        pool_weight,
        preferred_element_type=jnp.float32,
    )
    pooled = (mixed.reshape(length, width_loc) * pool_gain).astype(jnp.bfloat16)
    cols = residual.shape[1]
    experts = n_sp * EXP_DEV
    slots_cap = length * TOPK * 3 // (2 * experts)
    ids = routes.reshape(-1)
    onehot = (ids[:, None] == jnp.arange(experts)[None, :]).astype(jnp.int32)
    rank = jnp.sum(onehot * (jnp.cumsum(onehot, axis=0) - 1), axis=1)
    slot = (ids * slots_cap + rank).reshape(length, TOPK)
    gain_cols = lax.dynamic_slice_in_dim(norm_gain, tp_index * cols, cols, 0)
    updated, normed = project(pooled, residual, gain_cols[None, :], out_weight)
    places_all = jnp.arange(experts * slots_cap)
    picks = [(slot[:, k : k + 1] == places_all[None, :]).astype(jnp.bfloat16) for k in range(TOPK)]
    send = lax.dot_general(
        sum(picks), normed, (((0,), (0,)), ((), ())), preferred_element_type=jnp.float32
    ).astype(jnp.bfloat16)
    returned = run_experts(
        send.reshape(n_sp // CORES, CORES, slots_cap, cols), w_gate[0], w_up[0], w_down[0]
    ).reshape(-1, cols)
    total = jnp.zeros((length, cols), jnp.float32)
    for k in range(TOPK):
        row = jnp.dot(picks[k], returned, preferred_element_type=jnp.float32)
        total = total + route_weights[:, k : k + 1] * row
    combined = updated.astype(jnp.float32) + total
    return combined.astype(jnp.bfloat16)


def solution(mesh):
    placed = (
        P("sp", "tp"),
        P("sp", "tp"),
        P("sp"),
        P("tp", None, None),
        P("tp"),
        P(None, "tp"),
        P(),
        P("sp", None),
        P("sp", None),
        P("sp", None, "tp"),
        P("sp", None, "tp"),
        P("sp", None, "tp"),
    )
    return jax.shard_map(
        shards, mesh=mesh, in_specs=placed, out_specs=P("sp", "tp"), check_vma=False
    )
```

time: 298 us -> 161 us (0.54)
  waiting for transfers between devices: 175 us -> 0.01 us
  Pallas kernels: 0 us -> 133 us
  blocking collectives: 51.2 us -> 0 us
  matrix products: 25.1 us -> 8.79 us
  between operations: 13.4 us -> 0.2 us
  local copies, waits for them, and re-layouts: 12.1 us -> 4.6 us
  starting transfers between devices: 12 us -> 6.96 us
  other arithmetic: 8.74 us -> 5.53 us
    all_gather x3 -> x0, waiting for transfers between devices: 138 us -> none  [the longest x1 67.9 us: shards(): piece = lax.all_gather(part_rows, 'tp', axis=1, tiled=True)]
    pallas_call x0 -> x2, Pallas kernels: none -> 133 us  [the longest x1 111 us: run_experts(): pl.pallas_call(functools.partial(experts_kernel, n_sp, n_tp), out_shape=j...]
    all_to_all x1 -> x0, blocking collectives: 42.3 us -> none  [shards(): lax.all_to_all(send.reshape(experts, slots_cap, cols), 'sp', split_axis=0...]
    all_to_all x1 -> x0, waiting for transfers between devices: 37.6 us -> none  [shards(): lax.all_to_all(produced.reshape(n_sp, slots_cap, cols), 'sp', split_axis=...]
    dot_general x4 -> x3, matrix products: 22.9 us -> 6.58 us  [the longest x2 3.63 us: shards(): row = jnp.dot(picks[k], returned, preferred_element_type=jnp.float32)]
    psum x1 -> x0, blocking collectives: 8.94 us -> none  [shards(): squares = lax.psum(jnp.sum(upf * upf, axis=1), 'tp')]
    scatter x1 -> x0, local copies, waits for them, and re-layouts: 6.62 us -> none  [shards(): jnp.zeros((experts * slots_cap, cols), jnp.bfloat16).at[slot]]
    all_to_all x1 -> x0, starting transfers between devices: 4.74 us -> none  [shards(): lax.all_to_all(produced.reshape(n_sp, slots_cap, cols), 'sp', split_axis=...]
  transfers between devices with their start and end apart: 6 -> 2, of which waited for: 4 -> 0; matrix products, arithmetic and copies ran while one was open for 1% -> 5% of each run, Pallas kernels for 0% -> 0%
where the time goes in v1:
time: 161 us; the launch traced here: 159 us
  Pallas kernels  133 us (83%)
  matrix products  8.79 us (5%)
  starting transfers between devices  6.96 us (4%)
  other arithmetic  5.53 us (3%)
  local copies, waits for them, and re-layouts  4.6 us (3%)
    pallas_call x1, Pallas kernels, run_experts(): pl.pallas_call(functools.partial(experts_kernel, n_sp, n_tp), out_shape=j...  111 us
    pallas_call x1, Pallas kernels, project(): pl.pallas_call(functools.partial(project_kernel, n_tp), out_shape=[jax.Sh...  21.9 us
    ppermute x2, starting transfers between devices, shifted_2(): return lax.ppermute(shard, axis, pairs)  6.96 us
    dot_general x2, matrix products, shards(): row = jnp.dot(picks[k], returned, preferred_element_type=jnp.float32)  3.63 us
  transfers between devices with their start and end apart: 2, of which 0 were waited for; matrix products, arithmetic and copies ran while one was open for 5% of the time, Pallas kernels for 0%

profile of v1, /device:TPU:0, one launch (start us, length us, event | category | flops | bytes accessed | tf_op | source)
XLA Modules:
  0.0 158.6 jit_solution(13834093094339627772)
XLA Ops:
  0.0 0.0 copy-start
  0.0 0.8 fusion.45
  0.8 0.1 slice.121
  0.8 2.4 %collective-permute-start.1 = (bf16[15]{0:T(256)(128)(2,1)S(1)}, bf16[15]{0:T(256)(128)(2,1)S(1)}, u32[]{:S(2)}, u32[]{:S(2)}) collective-permute-start(bf16[15]{0:T(256)(128)(2,1)S(1)} %slice.121), channel_id=1, source_target_pairs={{0,4},{4,8},{8,12},{12,16},{16,20},{20,24},{24,28},{1,5},{5,9},{9,... | collective-permute-start | bytes 98 | tf_op jit(solution)/shard_map/ppermute | solution.py:21
  3.2 0.7 slice.119
  4.0 4.6 %collective-permute-start = (bf16[15,512]{1,0:T(8,128)(2,1)S(1)}, bf16[15,512]{1,0:T(8,128)(2,1)S(1)}, u32[]{:S(2)}, u32[]{:S(2)}) collective-permute-start(bf16[15,512]{1,0:T(8,128)(2,1)S(1)} %slice.119), channel_id=1, source_target_pairs={{0,4},{4,8},{8,12},{12,16},{16,20},{20,24},{24,28},{1,5},{5,9},{9,... | collective-permute-start | bytes 46088 | tf_op jit(solution)/shard_map/ppermute | solution.py:21
  8.7 0.8 copy.33
  9.6 0.1 eq.125
  9.7 0.1 eq.121
  9.9 1.1 reduce-window.6
  11.0 0.2 slice_reduce_fusion
  11.3 0.1 fusion.34
  11.4 0.1 reduce_sum.12
  11.5 0.1 copy.35
  11.6 0.7 multiply_add_fusion.15
  12.3 0.8 fusion.43
  13.1 1.3 dynamic_slice.3
  14.3 0.0 collective-permute-done.1
  14.3 0.1 pad_maximum_fusion
  14.4 0.8 and_convert_fusion.14
  15.2 0.0 collective-permute-done
  15.2 1.0 maximum_convert_fusion
  16.2 0.0 copy-done
  16.2 0.0 copy-start.3
  16.3 2.2 %fusion.30 = f32[4,256,128]{1,2,0:T(8,128)S(1)} fusion(bf16[4,128,128]{2,1,0:T(8,128)(2,1)S(1)} %copy-done, f32[271,512]{1,0:T(8,128)S(1)} %maximum_convert_fusion, f32[512]{0:T(512)S(1)} %get-tuple-element.31, f32[256]{0:T(256)S(1)} %get-tuple-element.10, f32[512]{0:T(512)S(1)} %get-tuple-element.32, f32[256]{0:T(256)S(1)} %get-tuple-element.11, ...), kind=kOutput, calls=%fused_computation.66 | convolution fusion | flops 42074112 | bytes 9093120 | tf_op jit(solution)/shard_map/tgc,gcd->tgd/dot_general | solution.py:470
  18.5 0.2 copy.37
  18.7 0.0 copy-done.3
  18.7 0.7 multiply_convert_fusion.pooled
  19.4 21.9 %shard_map.118 = (bf16[256,1024]{1,0:T(8,128)(2,1)}, bf16[256,1024]{1,0:T(8,128)(2,1)}) custom-call(bf16[256,512]{1,0:T(8,128)(2,1)} %multiply_convert_fusion.pooled, bf16[256,1024]{1,0:T(8,128)(2,1)} %residual.1, f32[1,1024]{1,0:T(1,128)} %bitcast.37, bf16[2048,1024]{1,0:T(8,128)(2,1)} %weight_hbm.1), custom_call_target="tpu_custom_call" | custom-call | tf_op jit(solution)/shard_map/pallas_call | solution.py:372
  41.4 2.9 %convolution_convert_fusion = bf16[768,1024]{1,0:T(8,128)(2,1)} fusion(bf16[256,1024]{1,0:T(8,128)(2,1)} %get-tuple-element.8, s32[256]{0:T(256)S(1)} %bitcast.38, s32[256]{0:T(256)S(1)} %bitcast.41), kind=kOutput, calls=%fused_computation | convolution fusion | flops 405012480 | bytes 2099200 | tf_op jit(solution)/shard_map/dot_general | solution.py:488
  44.3 110.6 %shard_map.119 = bf16[4,2,96,1024]{3,2,1,0:T(8,128)(2,1)} custom-call(bf16[4,2,96,1024]{3,2,1,0:T(8,128)(2,1)} %bitcast.35, bf16[4096,512]{1,0:T(8,128)(2,1)} %bitcast.32, bf16[4096,512]{1,0:T(8,128)(2,1)} %bitcast.33, bf16[2048,1024]{1,0:T(8,128)(2,1)} %bitcast.34), custom_call_target="tpu_custom_call" | custom-call | tf_op jit(solution)/shard_map/pallas_call | solution.py:401
  154.9 0.0 copy-start.1
  154.9 0.0 copy-start.2
  154.9 2.2 %convolution_multiply_fusion.1 = f32[256,1024]{1,0:T(8,128)S(1)} fusion(bf16[768,1024]{1,0:T(8,128)(2,1)} %bitcast.30, f32[256]{0:T(256)S(1)} %bitcast.43, s32[256]{0:T(256)S(1)} %bitcast.42), kind=kOutput, calls=%fused_computation.4 | convolution fusion | flops 403111936 | bytes 2623488 | tf_op jit(solution)/shard_map/dot_general | solution.py:496
  157.1 0.0 copy-done.1
  157.1 0.0 copy-done.2
  157.1 1.5 fusion.2
  (13 shorter events, 0.2 us)
Async XLA Ops:
  0.0 16.2 %copy-start = (bf16[4,128,128]{2,1,0:T(8,128)(2,1)S(1)}, bf16[4,128,128]{2,1,0:T(8,128)(2,1)}, u32[]{:S(2)}) copy-start(bf16[4,128,128]{2,1,0:T(8,128)(2,1)} %param.15) | copy-start | bytes 393220
  0.8 13.5 %collective-permute-start.1 = (bf16[15]{0:T(256)(128)(2,1)S(1)}, bf16[15]{0:T(256)(128)(2,1)S(1)}, u32[]{:S(2)}, u32[]{:S(2)}) collective-permute-start(bf16[15]{0:T(256)(128)(2,1)S(1)} %slice.121), channel_id=1, source_target_pairs={{0,4},{4,8},{8,12},{12,16},{16,20},{20,24},{24,28},{1,5},{5,9},{9,... | collective-permute-start | bytes 98 | tf_op jit(solution)/shard_map/ppermute | solution.py:21
  4.0 11.2 %collective-permute-start = (bf16[15,512]{1,0:T(8,128)(2,1)S(1)}, bf16[15,512]{1,0:T(8,128)(2,1)S(1)}, u32[]{:S(2)}, u32[]{:S(2)}) collective-permute-start(bf16[15,512]{1,0:T(8,128)(2,1)S(1)} %slice.119), channel_id=1, source_target_pairs={{0,4},{4,8},{8,12},{12,16},{16,20},{20,24},{24,28},{1,5},{5,9},{9,... | collective-permute-start | bytes 46088 | tf_op jit(solution)/shard_map/ppermute | solution.py:21
  16.2 2.4 %copy-start.3 = (f32[512]{0:T(512)S(1)}, f32[512]{0:T(512)}, u32[]{:S(2)}) copy-start(f32[512]{0:T(512)} %param.16) | copy-start | bytes 6148
  154.9 2.2 %copy-start.1 = (bf16[4,2,96,1024]{3,2,1,0:T(8,128)(2,1)S(1)}, bf16[4,2,96,1024]{3,2,1,0:T(8,128)(2,1)}, u32[]{:S(2)}) copy-start(bf16[4,2,96,1024]{3,2,1,0:T(8,128)(2,1)} %shard_map.119) | copy-start | bytes 4718596
  154.9 2.2 %copy-start.2 = (bf16[256,1024]{1,0:T(8,128)(2,1)S(1)}, bf16[256,1024]{1,0:T(8,128)(2,1)}, u32[]{:S(2)}) copy-start(bf16[256,1024]{1,0:T(8,128)(2,1)} %get-tuple-element.7) | copy-start | bytes 1572868
